TPU v7x, 256 devices: a 4x2x16 block of a 4x16x16 slice. The times are simulated.
256 devices in a mesh: grp: 2 (over y), sp: 16 (over z), tp: 8 (over x, core).
Axes of the slice: x: 4, y: 2, z: 16, core: 2. Of those that a mesh axis runs over, the one named last changes fastest.
The devices are a block of a 4x16x16 slice.
Arguments:
- latents: bfloat16 [8192, 4, 2048], P(('sp', 'tp'), 'grp'), parts along dimension 1, may hold values from -6 to 6
- context: bfloat16 [1024, 4, 2048], P('sp', 'grp'), parts along dimension 1, may hold values from -6 to 6
- condition: float32 [4, 2048], P('grp', 'sp'), parts along dimension 0, may hold values from -6 to 6
- cond_context: float32 [2048], P('sp'), may hold values from -6 to 6
- w_shift: bfloat16 [2048, 2048], P('sp', 'tp'), may hold values from -0.125 to 0.125
- w_scale: bfloat16 [2048, 2048], P('sp', 'tp'), may hold values from -0.125 to 0.125
- w_gate: bfloat16 [2048, 2048], P('sp', 'tp'), may hold values from -0.375 to 0.375
- norm_gain: float32 [2048], replicated, may hold values from 0.1 to 1.9
- w_query: bfloat16 [2048, 1024], P(None, 'tp'), may hold values from -0.375 to 0.375
- w_key: bfloat16 [2048, 512], P(None, 'tp'), may hold values from -0.125 to 0.125
- w_value: bfloat16 [2048, 512], P(None, 'tp'), may hold values from -0.25 to 0.25
- sink_logit: float32 [16], P('tp'), may hold values from 6 to 240
- w_out: bfloat16 [1024, 2048], P('tp'), may hold values from -0.1875 to 0.1875
Outputs:
- refined: bfloat16 [8192, 4, 2048], P(('sp', 'tp'), 'grp'), parts along dimension 1
There are 2 independent parts, one for each index of `grp`. A program takes and returns all parts, laid end to end along the dimension named above; an argument that names none is the same for every part. Nothing has to cross between parts.
All inputs are finite; a program needn't handle non-finite values.
Results may differ from a plain program's by a relative error of at most 0.017.
Values may be sent and summed in bfloat16 or wider, within the bound.
A program may use at most 128 MiB of HBM per device.

v0:
```python
import jax
import jax.numpy as jnp
from jax import lax
from jax.sharding import Mesh
from jax.sharding import PartitionSpec as P

HEAD_DIM = 64
WINDOW = 128
GRID_W = 64
TP = ("tp_0", "tp_1")
SP_TP = ("sp", "tp_0", "tp_1")


EPS = 1e-06
THETA = 10000.0
BIG_NEG = -1e30


def from_everyone(x, axis):
    copies = jnp.broadcast_to(x, (lax.axis_size(axis), *x.shape))
    return lax.all_to_all(copies, axis, split_axis=0, concat_axis=0, tiled=True)


def of_everyone(x, axis):
    return from_everyone(x, axis).sum(axis=0)


def packed_total(arrays, axis):
    vector, at, outs = (jnp.concatenate([a.reshape(-1) for a in arrays]), 0, [])
    subtotal = of_everyone(vector, axis)
    for a in arrays:
        outs.append(subtotal[at : at + a.size].reshape(a.shape))
        at += a.size
    return tuple(outs)


def in_one_piece(arrays, axis, dim, along):
    widths = [a.shape[along] for a in arrays]
    both = jnp.concatenate(arrays, axis=along)
    filled = lax.all_gather(both, axis, axis=dim, tiled=True)
    return tuple(jnp.split(filled, [sum(widths[:k]) for k in range(1, len(widths))], axis=along))


def with_halo(cells, sides, width):
    for axis, dim in sides:
        count = lax.axis_size(axis)
        ends = count - 1
        head = lax.slice_in_dim(cells, 0, width, axis=dim)
        tail = lax.slice_in_dim(cells, cells.shape[dim] - width, cells.shape[dim], axis=dim)
        cells = jnp.concatenate(
            [
                lax.ppermute(tail, axis, [(i, (i + 1) % count) for i in range(ends)]),
                cells,
                lax.ppermute(head, axis, [((i + 1) % count, i) for i in range(ends)]),
            ],
            axis=dim,
        )
    return cells


def in_blocks(x, dim, devices):
    dims = x.shape
    tiles = x.reshape(*dims[:dim], devices, dims[dim] // devices, *dims[dim + 1 :])
    return jnp.moveaxis(tiles, dim, 0)


def joined_along(tiles, dim):
    tiles = jnp.moveaxis(tiles, 0, dim)
    dims = tiles.shape
    return tiles.reshape(*dims[:dim], dims[dim] * dims[dim + 1], *dims[dim + 2 :])


def moved_by_axis(tiles, axes, order):
    dims = [lax.axis_size(a) for a in axes]
    tiles = tiles.reshape(*dims, *tiles.shape[1:])
    for k in order:
        tiles = lax.all_to_all(tiles, axes[k], split_axis=k, concat_axis=k, tiled=True)
    return tiles.reshape(-1, *tiles.shape[len(axes) :])


def one_axis_at_a_time(x, axes, order, split_dim, concat_dim):
    tiles = in_blocks(x, split_dim, lax.axis_size(axes))
    return joined_along(moved_by_axis(tiles, axes, order), concat_dim)


def rotate_pairs(vectors, grid_row, grid_col, head_dim):
    quarter = head_dim // 4
    inverse = THETA ** (-jnp.arange(quarter, dtype=jnp.float32) / quarter)
    angles = jnp.concatenate([grid_row[:, None] * inverse, grid_col[:, None] * inverse], axis=-1)
    shape = (angles.shape[0],) + (1,) * (vectors.ndim - 2) + (head_dim // 2,)
    cosine = jnp.cos(angles).reshape(shape)
    sine = jnp.sin(angles).reshape(shape)
    first_half = vectors[..., : head_dim // 2]
    second_half = vectors[..., head_dim // 2 :]
    return jnp.concatenate(
        [first_half * cosine - second_half * sine, first_half * sine + second_half * cosine],
        axis=-1,
    )


def modulate(tokens_in, gain, shift_rows, scale_rows):
    upcast = tokens_in.astype(jnp.float32)
    normed = upcast * lax.rsqrt(jnp.mean(upcast * upcast, axis=-1, keepdims=True) + EPS)
    return (normed * gain * (1.0 + scale_rows) + shift_rows).astype(jnp.bfloat16)


def on_device(
    latents,
    context,
    condition,
    cond_context,
    w_shift,
    w_scale,
    w_gate,
    norm_gain,
    w_query,
    w_key,
    w_value,
    sink_logit,
    w_out,
):
    samples = latents.shape[1]
    model_width = latents.shape[2]
    n_tp = lax.axis_size(TP)
    n_sp = lax.axis_size("sp")
    local_rows = latents.shape[0]
    tokens = local_rows * n_tp
    local_heads = w_query.shape[1] // HEAD_DIM
    local_kv = w_key.shape[1] // HEAD_DIM
    per_group = local_heads // local_kv
    q_cols = local_heads * HEAD_DIM
    kv_cols = local_kv * HEAD_DIM
    w_whole = lax.all_gather(w_out, TP, axis=0, tiled=True)
    lifted = jax.nn.silu(jnp.concatenate([condition, cond_context[None, :]], axis=0)).astype(
        jnp.bfloat16
    )
    part_shift = jnp.dot(lifted, w_shift, preferred_element_type=jnp.float32)
    part_scale = jnp.dot(lifted, w_scale, preferred_element_type=jnp.float32)
    part_gate = jnp.dot(lifted, w_gate, preferred_element_type=jnp.float32)
    sum_shift, sum_scale, sum_gate = packed_total((part_shift, part_scale, part_gate), "sp")
    shift_all, scale_all, gate_all = in_one_piece((sum_shift, sum_scale, sum_gate), TP, 1, 0)
    normed = modulate(latents, norm_gain, shift_all[:samples][None], scale_all[:samples][None])
    w_joint = jnp.concatenate([w_query, w_key, w_value], axis=1)
    shard_rows = lax.all_gather(normed, TP, axis=0, tiled=True)
    row_count = shard_rows.shape[0]
    flat_rows = shard_rows.reshape(row_count * samples, model_width)
    projected = jnp.dot(flat_rows, w_joint, preferred_element_type=jnp.float32).reshape(
        row_count, samples, w_joint.shape[1]
    )
    offset = lax.axis_index("sp") * tokens
    positions = offset + jnp.arange(tokens, dtype=jnp.int32)
    grid_row = (positions // GRID_W).astype(jnp.float32)
    grid_col = (positions % GRID_W).astype(jnp.float32)
    queries = rotate_pairs(
        projected[..., :q_cols].reshape(tokens, samples, local_heads, HEAD_DIM),
        grid_row,
        grid_col,
        HEAD_DIM,
    ).astype(jnp.bfloat16)
    lat_keys = rotate_pairs(
        projected[..., q_cols : q_cols + kv_cols].reshape(tokens, samples, local_kv, HEAD_DIM),
        grid_row,
        grid_col,
        HEAD_DIM,
    ).astype(jnp.bfloat16)
    lat_values = projected[..., q_cols + kv_cols :].astype(jnp.bfloat16)
    paired = jnp.concatenate([lat_keys.reshape(tokens, samples, kv_cols), lat_values], axis=-1)
    extended = with_halo(paired, (("sp", 0),), WINDOW)
    w_pair = jnp.concatenate([w_key, w_value], axis=1)
    ctx_shift = shift_all[samples][None, None]
    ctx_scale = scale_all[samples][None, None]
    ctx_normed = modulate(context, norm_gain, ctx_shift, ctx_scale)
    row_count = context.shape[0]
    flat_ctx = ctx_normed.reshape(row_count * samples, model_width)
    ctx_pairs = lax.all_gather(
        jnp.dot(flat_ctx, w_pair, preferred_element_type=jnp.float32)
        .astype(jnp.bfloat16)
        .reshape(row_count, samples, 2 * kv_cols),
        "sp",
        axis=0,
        tiled=True,
    )
    ctx_len = ctx_pairs.shape[0]
    ctx_keys = ctx_pairs[..., :kv_cols].reshape(ctx_len, samples, local_kv, HEAD_DIM)
    ctx_values = ctx_pairs[..., kv_cols:].reshape(ctx_len, samples, local_kv, HEAD_DIM)
    block_rows = min(tokens, 512)
    n_blocks = tokens // block_rows
    seq_length = tokens * n_sp
    head_sinks = sink_logit.reshape(local_kv, per_group)[None, :, :, None]
    score_scale = HEAD_DIM ** (-0.5)

    def attend_block(block_index):
        first_row = block_index * block_rows
        q_blk = queries.reshape(block_rows, samples, local_kv, per_group, HEAD_DIM)
        k_blk = extended[..., :kv_cols].reshape(
            block_rows + 2 * WINDOW, samples, local_kv, HEAD_DIM
        )
        v_blk = extended[..., kv_cols:].reshape(
            block_rows + 2 * WINDOW, samples, local_kv, HEAD_DIM
        )
        lat_scores = (
            jnp.einsum("qsngd,ksnd->sngqk", q_blk, k_blk, preferred_element_type=jnp.float32)
            * score_scale
        )
        q_pos = offset + first_row + jnp.arange(block_rows, dtype=jnp.int32)
        k_pos = offset + first_row - WINDOW + jnp.arange(block_rows + 2 * WINDOW, dtype=jnp.int32)
        in_window = (
            (jnp.abs(q_pos[:, None] - k_pos[None, :]) <= WINDOW)
            & (k_pos >= 0)[None, :]
            & (k_pos < seq_length)[None, :]
        )
        lat_scores = jnp.where(in_window, lat_scores, BIG_NEG)
        ctx_scores = (
            jnp.einsum("qsngd,ksnd->sngqk", q_blk, ctx_keys, preferred_element_type=jnp.float32)
            * score_scale
        )
        row_max = jnp.maximum(
            jnp.maximum(jnp.max(lat_scores, axis=-1), jnp.max(ctx_scores, axis=-1)), head_sinks
        )
        lat_exp = jnp.exp(lat_scores - row_max[..., None])
        ctx_exp = jnp.exp(ctx_scores - row_max[..., None])
        denominator = (
            jnp.sum(lat_exp, axis=-1) + jnp.sum(ctx_exp, axis=-1) + jnp.exp(head_sinks - row_max)
        )
        lat_weights = (lat_exp / denominator[..., None]).astype(jnp.bfloat16)
        ctx_weights = (ctx_exp / denominator[..., None]).astype(jnp.bfloat16)
        summed = jnp.einsum(
            "sngqk,ksnd->qsngd", lat_weights, v_blk, preferred_element_type=jnp.float32
        )
        summed = summed + jnp.einsum(
            "sngqk,ksnd->qsngd", ctx_weights, ctx_values, preferred_element_type=jnp.float32
        )
        return summed.astype(jnp.bfloat16).reshape(block_rows, samples, q_cols)

    attended = lax.map(attend_block, jnp.arange(n_blocks)).reshape(tokens * samples, q_cols)
    own_heads = one_axis_at_a_time(attended, TP, (1, 0), 0, 1)
    grouped = own_heads.reshape(local_rows * samples, n_tp, q_cols)
    w_groups = w_whole.reshape(n_tp, q_cols, model_width)
    partials = jnp.einsum("rgc,gcd->grd", grouped, w_groups, preferred_element_type=jnp.float32)
    summed_out = jnp.sum(partials.astype(jnp.bfloat16).astype(jnp.float32), axis=0)
    mixed = summed_out.reshape(local_rows, samples, model_width)
    refined = latents.astype(jnp.float32) + gate_all[:samples][None] * mixed
    return refined.astype(jnp.bfloat16)


def solution(mesh):
    finer = Mesh(
        mesh.devices.reshape(mesh.shape["grp"], mesh.shape["sp"], 4, 2),
        ("grp", "sp", "tp_0", "tp_1"),
    )
    return jax.shard_map(
        on_device,
        mesh=finer,
        in_specs=(
            P(SP_TP, "grp", None),
            P("sp", "grp", None),
            P("grp", "sp"),
            P("sp"),
            P("sp", TP),
            P("sp", TP),
            P("sp", TP),
            P(),
            P(None, TP),
            P(None, TP),
            P(None, TP),
            P(TP),
            P(TP, None),
        ),
        out_specs=P(SP_TP, "grp", None),
        check_vma=False,
    )
```

profile of v0, /device:TPU:33, one launch (start us, length us, event | category | flops | bytes accessed | tf_op | source)
XLA Modules:
  0.0 152.9 jit_solution(1924405531050254063)
XLA Ops:
  6.5 0.0 copy-start
  6.6 0.0 copy-start.3
  6.6 0.0 copy-start.4
  6.6 0.8 copy-done
  7.4 0.8 fusion.62
  8.2 1.0 fusion.64
  9.2 1.0 fusion.66
  10.3 0.7 broadcast_in_dim.21
  11.0 24.5 %all-to-all-start = ((f32[16,1,2304]{2,1,0:T(1,128)}), f32[16,1,2304]{2,1,0:T(1,128)S(1)}, u32[]{:S(2)}, u32[]{:S(2)}) async-start(f32[16,1,2304]{2,1,0:T(1,128)} %broadcast_in_dim.21), calls=%async_computation | async-start | bytes 294912 | tf_op jit(solution)/shard_map/all_to_all | solution.py:21
  35.5 0.1 all-gather.3.cloned.1.call-start
  35.6 1.3 fusion.20
  36.9 1.3 fusion.25
  38.2 9.2 %all-to-all-done = f32[16,1,2304]{2,1,0:T(1,128)S(1)} async-done(((f32[16,1,2304]{2,1,0:T(1,128)}), f32[16,1,2304]{2,1,0:T(1,128)S(1)}, u32[]{:S(2)}, u32[]{:S(2)}) %all-to-all-start) | async-done | bytes 147488 | tf_op jit(solution)/shard_map/all_to_all | solution.py:21
  47.4 0.1 reduce_sum.56
  47.6 17.4 %all_gather.12 = f32[9,2048]{1,0:T(8,128)S(1)} all-gather(f32[9,256]{1,0:T(8,128)S(1)} %pad_maximum_fusion.8), channel_id=1, replica_groups=mesh['grp'=2,'sp'=16,'tp_0'=4,'tp_1'=2] {'tp_0','tp_1'}, dimensions={1}, use_global_device_ids=true | all-gather | bytes 82944 | tf_op jit(solution)/shard_map/all_gather | solution.py:40
  65.0 2.7 %fusion.29 = (bf16[64,2,2048]{2,0,1:T(8,128)(2,1)}, bf16[64,2,2048]{2,0,1:T(8,128)(2,1)S(1)}) fusion(f32[2,2048]{1,0:T(2,128)S(1)} %get-tuple-element.38, f32[2,2048]{1,0:T(2,128)S(1)} %get-tuple-element.39, f32[2048]{0:T(1024)} %param.20, f32[64,2]{0,1:T(2,128)S(1)} %get-tuple-element.56, bf16[64,2,2048]{2,1,0:T(2,128)(2,1)} %param.13, ...), kind=kLoop, calls=%fused_computation.37 | loop fusion | flops 3145728 | bytes 2155520 | tf_op jit(solution)/shard_map/convert_element_type | solution.py:104
  67.7 0.1 all-gather.3.cloned.1.call-update
  67.7 0.1 all-gather.5.cloned.1.call-start
  67.8 0.7 all-gather.5.cloned.1.call-update
  68.6 0.1 broadcast_multiply_fusion.1
  68.7 1.2 copy.72
  69.9 0.2 fusion.46
  70.2 0.8 fusion.10
  71.0 0.5 copy.74
  71.5 0.2 reshape.288
  71.7 0.0 copy-done.3
  71.7 0.0 copy-done.4
  71.7 0.3 convolution_convert_fusion
  72.0 26.0 %all_gather.14 = bf16[1024,2,128]{2,1,0:T(2,128)(2,1)S(1)} all-gather(bf16[64,2,128]{2,1,0:T(2,128)(2,1)S(1)} %bitcast.105), channel_id=1, replica_groups=mesh['grp'=2,'sp'=16,'tp_0'=4,'tp_1'=2] {'sp'}, dimensions={0}, use_global_device_ids=true | all-gather | bytes 557056 | tf_op jit(solution)/shard_map/all_gather | solution.py:175
  98.1 0.9 fusion.68
  99.0 0.4 copy.94
  99.4 0.4 copy.95
  99.8 0.0 all-gather.3.cloned.1.call-done
  99.9 3.5 %fusion.31 = f32[512,2,256]{0,2,1:T(8,128)S(1)} fusion(bf16[512,2,2048]{2,0,1:T(8,128)(2,1)} %all-gather.3.cloned.1.call-done, bf16[2048,64]{0,1:T(8,128)(2,1)S(1)} %copy-done.3, bf16[2048,64]{0,1:T(8,128)(2,1)S(1)} %copy-done.4, bf16[2048,128]{0,1:T(8,128)(2,1)S(1)} %copy.72), kind=kOutput, calls=%fused_computation.40 | convolution fusion | flops 1076887552 | bytes 6291456 | tf_op jit(solution)/shard_map/dot_general | solution.py:147
  103.5 1.3 collective-permute-start.1
  104.8 4.2 %collective-permute-start = (bf16[128,2,128]{0,2,1:T(8,128)(2,1)S(1)}, bf16[128,2,128]{0,2,1:T(8,128)(2,1)S(1)}, u32[]{:S(2)}, u32[]{:S(2)}) collective-permute-start(bf16[128,2,128]{0,2,1:T(8,128)(2,1)S(1)} %get-tuple-element.34), channel_id=1, source_target_pairs={{0,8},{8,16},{16,24},{24,32},{32,40},{40,48},{48,56},{56,64},{64,7... | collective-permute-start | bytes 196616 | tf_op jit(solution)/shard_map/ppermute | solution.py:52
  109.0 0.1 subtract_convert_fusion
  109.1 1.3 bitcast_reduce_fusion
  110.4 0.0 copy-start.2
  110.5 0.0 collective-permute-done.1
  110.5 0.0 collective-permute-done
  110.5 1.3 fusion.3
  111.8 0.0 copy-done.2
  111.8 0.1 maximum_maximum_fusion
  111.9 1.4 fusion.1
  113.3 1.4 fusion.2
  114.6 0.1 exponential_add_fusion
  114.7 1.9 %fusion.4 = f32[2,64,2,512]{3,1,2,0:T(8,128)S(1)} fusion(f32[2,1024,512,2]{2,1,3,0:T(8,128)S(1)} %get-tuple-element.54, f32[2,2,512]{2,1,0:T(2,128)S(1)} %exponential_add_fusion, f32[2,2,512]{2,1,0:T(2,128)S(1)} %maximum_maximum_fusion, bf16[1024,2,64]{0,2,1:T(8,128)(2,1)S(1)} %copy.95), kind=kOutput, calls=%fused_computation.11 | convolution fusion | flops 276824064 | bytes 9191424 | tf_op jit(solution)/shard_map/while/body/eval_jaxpr/sngqk,ksnd->qsngd/dot_general | solution.py:230
  116.7 2.0 %fusion.17 = bf16[512,2,1,2,64]{0,4,3,1,2:T(8,128)(2,1)S(1)} fusion(f32[2,64,2,512]{3,1,2,0:T(8,128)S(1)} %fusion.4, f32[2,2,512]{2,1,0:T(2,128)S(1)} %exponential_add_fusion, f32[2,2,512]{2,1,0:T(2,128)S(1)} %maximum_maximum_fusion, f32[2,768,512,2]{2,1,3,0:T(8,128)S(1)} %get-tuple-element.52, pred[512,768]{0,1:T(8,128)(4,1)S(1)} %fusion.10, ...), kind=kOutput, calls=%fused_computation.26 | convolution fusion | flops 209453056 | bytes 7684096 | tf_op jit(solution)/shard_map/while/body/eval_jaxpr/sngqk,ksnd->qsngd/dot_general | solution.py:227
  118.7 0.4 copy.79
  119.1 0.2 reshape_reshape_reshape.3
  119.4 0.0 copy-start.1
  119.4 10.4 %all_to_all.16 = bf16[4,2,128,128]{3,2,0,1:T(8,128)(2,1)S(1)} all-to-all(bf16[4,2,128,128]{3,2,0,1:T(8,128)(2,1)S(1)} %copy.80), channel_id=1, replica_groups=mesh['grp'=2,'sp'=16,'tp_0'=4,'tp_1'=2] {'tp_1'}, dimensions={1} | all-to-all | bytes 524288 | tf_op jit(solution)/shard_map/all_to_all | solution.py:77
  129.8 0.7 copy.81
  130.5 3.6 %all-to-all-start.2 = ((bf16[4,2,128,128]{3,2,1,0:T(8,128)(2,1)}), bf16[4,2,128,128]{3,2,1,0:T(8,128)(2,1)S(1)}, u32[]{:S(2)}, u32[]{:S(2)}) async-start(bf16[4,2,128,128]{3,2,1,0:T(8,128)(2,1)} %copy.81), calls=%async_computation.2 | async-start | bytes 524288 | tf_op jit(solution)/shard_map/all_to_all | solution.py:77
  134.1 5.4 %all-gather.5.cloned.1.call-done = bf16[1024,2048]{1,0:T(8,128)(2,1)} async-done(((bf16[128,2048]{1,0:T(8,128)(2,1)}), bf16[1024,2048]{1,0:T(8,128)(2,1)}) %all-gather.5.cloned.1.call-update) | async-done | bytes 4194320 | tf_op jit(solution)/shard_map/all_gather | solution.py:133
  139.5 0.4 all-to-all-done.2
  139.9 3.5 %convert_reduce_fusion = f32[128,2048]{1,0:T(8,128)S(1)} fusion(bf16[128,8,128]{2,0,1:T(8,128)(2,1)S(1)} %bitcast.102, bf16[8,128,2048]{2,1,0:T(8,128)(2,1)} %bitcast.100), kind=kOutput, calls=%fused_computation.3 | convolution fusion | flops 542900224 | bytes 5505024 | tf_op jit(solution)/shard_map/rgc,gcd->grd/dot_general | solution.py:239
  143.4 0.6 reshape.294
  144.0 0.0 copy-done.1
  144.0 0.7 fusion.30
  144.7 1.3 copy.83
  (24 shorter events, 0.4 us)
Async XLA Ops:
  6.5 0.8 copy-start
  6.6 65.2 %copy-start.3 = (bf16[2048,64]{0,1:T(8,128)(2,1)S(1)}, bf16[2048,64]{0,1:T(8,128)(2,1)}, u32[]{:S(2)}) copy-start(bf16[2048,64]{0,1:T(8,128)(2,1)} %param.23) | copy-start | bytes 786436
  6.6 65.2 %copy-start.4 = (bf16[2048,64]{0,1:T(8,128)(2,1)S(1)}, bf16[2048,64]{0,1:T(8,128)(2,1)}, u32[]{:S(2)}) copy-start(bf16[2048,64]{0,1:T(8,128)(2,1)} %param.22) | copy-start | bytes 786436
  11.0 36.4 %all-to-all-start = ((f32[16,1,2304]{2,1,0:T(1,128)}), f32[16,1,2304]{2,1,0:T(1,128)S(1)}, u32[]{:S(2)}, u32[]{:S(2)}) async-start(f32[16,1,2304]{2,1,0:T(1,128)} %broadcast_in_dim.21), calls=%async_computation | async-start | bytes 294912 | tf_op jit(solution)/shard_map/all_to_all | solution.py:21
  35.5 64.3 %all-gather.3.cloned.1.call-start = ((), (), s32[]{:S(2)}) async-start(), calls=%async_computation.3 | async-start | bytes 4718592 | tf_op jit(solution)/shard_map/all_gather | solution.py:144
  67.7 71.7 %all-gather.5.cloned.1.call-start = ((), (), s32[]{:S(2)}) async-start(), calls=%async_computation.4 | async-start | bytes 4718592 | tf_op jit(solution)/shard_map/all_gather | solution.py:133
  103.5 7.0 %collective-permute-start.1 = (bf16[128,2,128]{0,2,1:T(8,128)(2,1)S(1)}, bf16[128,2,128]{0,2,1:T(8,128)(2,1)S(1)}, u32[]{:S(2)}, u32[]{:S(2)}) collective-permute-start(bf16[128,2,128]{0,2,1:T(8,128)(2,1)S(1)} %get-tuple-element.36), channel_id=1, source_target_pairs={{8,0},{16,8},{24,16},{32,24},{40,32},{48,40},{56,48},{64,56},{72,6... | collective-permute-start | bytes 196616 | tf_op jit(solution)/shard_map/ppermute | solution.py:54
  104.8 5.6 %collective-permute-start = (bf16[128,2,128]{0,2,1:T(8,128)(2,1)S(1)}, bf16[128,2,128]{0,2,1:T(8,128)(2,1)S(1)}, u32[]{:S(2)}, u32[]{:S(2)}) collective-permute-start(bf16[128,2,128]{0,2,1:T(8,128)(2,1)S(1)} %get-tuple-element.34), channel_id=1, source_target_pairs={{0,8},{8,16},{16,24},{24,32},{32,40},{40,48},{48,56},{56,64},{64,7... | collective-permute-start | bytes 196616 | tf_op jit(solution)/shard_map/ppermute | solution.py:52
  110.4 1.4 copy-start.2
  119.4 24.6 %copy-start.1 = (bf16[64,2,2048]{2,1,0:T(2,128)(2,1)S(1)}, bf16[64,2,2048]{2,1,0:T(2,128)(2,1)}, u32[]{:S(2)}) copy-start(bf16[64,2,2048]{2,1,0:T(2,128)(2,1)} %param.13) | copy-start | bytes 1572868
  130.5 9.4 %all-to-all-start.2 = ((bf16[4,2,128,128]{3,2,1,0:T(8,128)(2,1)}), bf16[4,2,128,128]{3,2,1,0:T(8,128)(2,1)S(1)}, u32[]{:S(2)}, u32[]{:S(2)}) async-start(bf16[4,2,128,128]{3,2,1,0:T(8,128)(2,1)} %copy.81), calls=%async_computation.2 | async-start | bytes 524288 | tf_op jit(solution)/shard_map/all_to_all | solution.py:77
Sparse Core Ops, SparseCore 0:
  67.9 31.4 all-gather.2
  101.3 38.1 all-gather.4
where the time goes:
time: 154 us; the launch traced here: 153 us
  blocking collectives  53.8 us (35%)
  starting transfers between devices  33.8 us (22%)
  matrix products  16.6 us (11%)
  waiting for transfers between devices  15.8 us (10%)
  between operations  13.8 us (9%)
  other arithmetic  10.3 us (7%)
  local copies, waits for them, and re-layouts  8.78 us (6%)
    all_gather x1, blocking collectives, on_device(): lax.all_gather(jnp.dot(flat_ctx, w_pair, preferred_element_type=jnp.float...  26 us
    all_to_all x1, starting transfers between devices, from_everyone(): return lax.all_to_all(copies, axis, split_axis=0, concat_axis=0, tiled=True)  24.5 us
    all_gather x1, blocking collectives, in_one_piece(): filled = lax.all_gather(both, axis, axis=dim, tiled=True)  17.4 us
    all_to_all x1, blocking collectives, moved_by_axis(): lax.all_to_all(tiles, axes[k], split_axis=k, concat_axis=k, tiled=True)  10.4 us
    all_to_all x1, waiting for transfers between devices, from_everyone(): return lax.all_to_all(copies, axis, split_axis=0, concat_axis=0, tiled=True)  9.2 us
    all_gather x1, waiting for transfers between devices, on_device(): w_whole = lax.all_gather(w_out, TP, axis=0, tiled=True)  5.39 us
    ppermute x1, starting transfers between devices, with_halo(): lax.ppermute(tail, axis, [(i, (i + 1) % count) for i in range(ends)])  4.22 us
    all_to_all x1, starting transfers between devices, moved_by_axis(): lax.all_to_all(tiles, axes[k], split_axis=k, concat_axis=k, tiled=True)  3.59 us
  transfers between devices with their start and end apart: 6, of which 3 were waited for; matrix products, arithmetic and copies ran while one was open for 15% of the time, Pallas kernels for 0%

commit v1 on v0

v1 whole, which is shorter than its diff:
```python
import functools
import math

import jax
import jax.numpy as jnp
import numpy as np
from jax import lax
from jax.experimental import pallas as pl
from jax.experimental.pallas import tpu as pltpu
from jax.sharding import PartitionSpec as P

HEAD_DIM = 64
WINDOW = 128
GRID_W = 64
EPS = 1e-06
THETA = 10000.0
BIG_NEG = -1e30
LOG2E = math.log2(math.e)
MESH = pl.DeviceIdType.MESH
F32 = jnp.float32
BF16 = jnp.bfloat16
LAT_SPLIT = 96


def rope_tables(n_rows):
    quarter = HEAD_DIM // 4
    inverse = (THETA ** (-np.arange(quarter, dtype=np.float32) / np.float32(quarter))).astype(np.float32)
    lane = np.arange(128)
    freq = inverse[lane % quarter]
    by_row = (lane % (HEAD_DIM // 2)) < quarter
    sign = np.where(lane % HEAD_DIM < HEAD_DIM // 2, -1.0, 1.0)

    def tables(positions, mine):
        angle = (positions.astype(np.float32)[:, None] * freq[None, :]).astype(np.float64)
        cosine = np.where(mine[None, :], np.cos(angle), 0.0)
        sine = np.where(mine[None, :], np.sin(angle) * sign[None, :], 0.0)
        return cosine, sine

    def four(positions, mine, ones):
        cosine, sine = tables(positions, mine)
        scale = HEAD_DIM ** (-0.5) * LOG2E
        key = (lane < HEAD_DIM)[None, :]
        return np.stack(
            [cosine * scale, sine * scale, np.where(key, cosine, ones), np.where(key, sine, 0.0)]
        ).astype(np.float32)

    cols = np.repeat(np.arange(GRID_W), 2)
    return four(cols, ~by_row, 1.0), four(np.arange(n_rows), by_row, 0.0)


def remote(src, dst, send_sem, recv_sem, device):
    return pltpu.make_async_remote_copy(
        src_ref=src,
        dst_ref=dst,
        send_sem=send_sem,
        recv_sem=recv_sem,
        device_id=device,
        device_id_type=MESH,
    )


class TwoHopGather:
    def __init__(self, n, me, slot, send_sems, recv_sems):
        self.n, self.me, self.slot = n, me, slot
        self.send_sems, self.recv_sems = send_sems, recv_sems
        self.reach = {1: n // 2, -1: n - 1 - n // 2}
        self.sent, self.pending = [], {}
        for way in (1, -1):
            for e in range(1, self.reach[way] + 1):
                self.pending[(way, e)] = True

    def at(self, way, e):
        return e - 1 if way == 1 else self.reach[1] + e - 1

    def send(self, way, d, e):
        owner = lax.rem(self.me - way * d + self.n, self.n)
        target = lax.rem(self.me + way * (e - d) + self.n, self.n)
        k = self.at(way, e)
        copy = remote(
            self.slot(owner), self.slot(owner), self.send_sems.at[k], self.recv_sems.at[k], {"sp": target}
        )
        copy.start()
        self.sent.append(copy)

    def pass_on(self, d):
        for way in (1, -1):
            if d >= self.reach[way]:
                continue
            if d > 0:
                self.wait(way, d)
            for e in (d + 1, d + 2):
                if e <= self.reach[way]:
                    self.send(way, d, e)

    def wait(self, way, e):
        owner = lax.rem(self.me - way * e + self.n, self.n)
        k = self.at(way, e)
        remote(
            self.slot(owner), self.slot(owner), self.send_sems.at[k], self.recv_sems.at[k], {"sp": self.me}
        ).wait_recv()
        del self.pending[(way, e)]

    def finish(self):
        for way, e in list(self.pending):
            self.wait(way, e)

    def drain(self):
        for copy in self.sent:
            copy.wait_send()


class RingOfChips:
    def __init__(self, buf, me, n, send_sems, recv_sems, pieces):
        self.buf, self.n = buf, n
        self.send_sems, self.recv_sems = send_sems, recv_sems
        self.pieces = pieces
        self.x, self.c = me // 2, lax.rem(me, 2)
        self.chips = n // 2
        self.me = me
        self.partner = me + 1 - 2 * self.c
        self.left_x = lax.rem(self.x + self.chips - 1, self.chips)
        self.right_x = lax.rem(self.x + 1, self.chips)
        self.far_x = lax.rem(self.x + 2, self.chips)
        self.sent = []
        self.base = {}
        k = 0
        for name in ("left", "right"):
            self.base[name] = k
            k += len(pieces)
        for name in ("far", "own2", "left2", "right2", "far2"):
            self.base[name] = k
            k += 1

    @staticmethod
    def count(pieces):
        return 2 * len(pieces) + 5

    def piece(self, owner, p):
        lo, size = self.pieces[p]
        return self.buf.at[owner, pl.ds(lo, size), :]

    def go(self, ref, k, target):
        copy = remote(ref, ref, self.send_sems.at[k], self.recv_sems.at[k], {"tp": target})
        copy.start()
        self.sent.append(copy)

    def land(self, ref, k):
        remote(ref, ref, self.send_sems.at[k], self.recv_sems.at[k], {"tp": self.partner}).wait_recv()

    def send_own(self, p):
        ref = self.piece(self.me, p)
        self.go(ref, self.base["left"] + p, self.right_x * 2 + self.c)
        self.go(ref, self.base["right"] + p, self.left_x * 2 + self.c)

    def share_own(self):
        self.go(self.buf.at[self.me], self.base["own2"], self.partner)

    def pass_near(self):
        left, right = self.left_x * 2 + self.c, self.right_x * 2 + self.c
        for p in range(len(self.pieces)):
            self.land(self.piece(left, p), self.base["left"] + p)
            self.land(self.piece(right, p), self.base["right"] + p)
        from_x = lax.rem(self.x + self.chips - 1 + 2 * self.c, self.chips)
        to_x = lax.rem(self.x + self.chips + 1 - 2 * self.c, self.chips)
        self.go(self.buf.at[from_x * 2 + self.c], self.base["far"], to_x * 2 + self.c)
        self.go(self.buf.at[left], self.base["left2"], self.partner)
        self.go(self.buf.at[right], self.base["right2"], self.partner)

    def pass_far(self):
        far = self.far_x * 2 + self.c
        self.land(self.buf.at[far], self.base["far"])
        self.go(self.buf.at[far], self.base["far2"], self.partner)

    def land_shared(self, name):
        x = {"own2": self.x, "left2": self.left_x, "right2": self.right_x, "far2": self.far_x}[name]
        self.land(self.buf.at[x * 2 + 1 - self.c], self.base[name])

    def drain(self):
        for copy in self.sent:
            copy.wait_send()


def kernel(
    n_sp, n_tp, seq_length,
    lat_hbm, ctx_hbm, cond_hbm, cc_hbm, wsh_hbm, wsc_hbm, wga_hbm, gain_hbm, wq_hbm, wkt_hbm, wvt_hbm, sink_ref,
    wo_hbm, col_hbm, row_hbm,
    out_ref,
    lat_all, wo_all, ctx_v, cond_v, cc_v, wmod_v, gain_v, w_all, wkvt_v, col_v, row_v,
    pm, ms, a16, b16, g16, ac16, bc16, ssq, rsb, rsc, xn, tmp,
    q_s, kv_s, vv_s, ck, cv, o_s, m_s, tmp2, asend, att_all,
    loc, zsend, zrecv, lsend, lrecv, wsend, wrecv, msend, mrecv, hsend, hrecv, asem, arecv,
):
    sp = lax.axis_index("sp")
    tp = lax.axis_index("tp")
    rows = lat_all.shape[1]
    local_tok = rows // 2
    tokens = local_tok * n_tp
    width = lat_all.shape[2]
    mod_cols = pm.shape[2]
    ctx_tok = ctx_v.shape[0] // 2

    lat_x = RingOfChips(lat_all, tp, n_tp, lsend, lrecv, ((0, LAT_SPLIT), (LAT_SPLIT, rows - LAT_SPLIT)))
    wo_x = RingOfChips(wo_all, tp, n_tp, wsend, wrecv, ((0, rows),))
    mods = TwoHopGather(n_sp, sp, lambda o: pm.at[o], zsend.at[0], zrecv.at[0])
    ctxs = TwoHopGather(
        n_sp, sp, lambda o: ck.at[:, pl.ds(pl.multiple_of(o * ctx_tok, ctx_tok), ctx_tok), :], zsend.at[1], zrecv.at[1]
    )

    barrier = pltpu.get_barrier_semaphore()
    near = [d for d in (1, 2, n_sp - 1, n_sp - 2)]
    for d in near:
        pl.semaphore_signal(barrier, inc=1, device_id={"sp": lax.rem(sp + d, n_sp)}, device_id_type=MESH)
    for k in range(1, n_tp):
        pl.semaphore_signal(barrier, inc=1, device_id={"tp": lax.rem(tp + k, n_tp)}, device_id_type=MESH)

    loads = [
        pltpu.make_async_copy(cond_hbm, cond_v, loc.at[0]),
        pltpu.make_async_copy(cc_hbm, cc_v, loc.at[1]),
        pltpu.make_async_copy(wsh_hbm, wmod_v.at[0], loc.at[2]),
        pltpu.make_async_copy(wsc_hbm, wmod_v.at[1], loc.at[3]),
        pltpu.make_async_copy(wga_hbm, wmod_v.at[2], loc.at[4]),
        pltpu.make_async_copy(lat_hbm, lat_all.at[tp], loc.at[5]),
        pltpu.make_async_copy(wkt_hbm, wkvt_v.at[pl.ds(0, HEAD_DIM)], loc.at[6]),
        pltpu.make_async_copy(wvt_hbm, wkvt_v.at[pl.ds(HEAD_DIM, HEAD_DIM)], loc.at[7]),
        pltpu.make_async_copy(wq_hbm, w_all.at[:, pl.ds(0, 128)], loc.at[8]),
        pltpu.make_async_copy(ctx_hbm, ctx_v, loc.at[9]),
        pltpu.make_async_copy(gain_hbm, gain_v, loc.at[10]),
        pltpu.make_async_copy(col_hbm, col_v, loc.at[11]),
        pltpu.make_async_copy(row_hbm.at[:, pl.ds(pl.multiple_of(sp * n_tp, n_tp), n_tp), :], row_v, loc.at[12]),
        pltpu.make_async_copy(wo_hbm, wo_all.at[tp], loc.at[13]),
    ]
    for load in loads:
        load.start()

    for load in loads[:5]:
        load.wait()
    sub = lax.broadcasted_iota(jnp.int32, (8, cond_v.shape[1]), 0)
    kind = lax.rem(sub, 3)
    raw = jnp.where(kind == 0, cond_v[0:1, :], jnp.where(kind == 1, cond_v[1:2, :], cc_v[0:1, :]))
    lifted = raw / (1.0 + jnp.exp(-raw))
    part = jnp.zeros((8, mod_cols), F32)
    for k in range(3):
        mine = (sub >= 3 * k) & (sub < 3 * k + 3)
        part = part + jnp.dot(
            jnp.where(mine, lifted, 0.0).astype(BF16), wmod_v[k], preferred_element_type=F32
        )
    pm[sp] = part

    pl.semaphore_wait(barrier, len(near) + n_tp - 1)
    mods.pass_on(0)
    loads[5].wait()
    lat_x.send_own(0)
    lat_x.share_own()
    for load in loads[6:]:
        load.wait()
    wo_x.share_own()

    w_all[:, 128:256] = wkvt_v[...].T
    mods.pass_on(2)

    def row_scale(load_rows, n_rows, rs_ref):
        def body(i, _):
            at = pl.ds(pl.multiple_of(i * 16, 16), 16)
            x = load_rows(at).astype(F32)
            sq = x * x
            acc = sq[:, 0:128]
            for k in range(1, width // 128):
                acc = acc + sq[:, 128 * k : 128 * k + 128]
            ssq[at, :] = acc
            return 0

        lax.fori_loop(0, n_rows // 16, body, 0)
        total = jnp.sum(ssq[0:n_rows, :], axis=-1, keepdims=True)
        rs_ref[0:n_rows, :] = jnp.broadcast_to(lax.rsqrt(total * (1.0 / width) + EPS), (n_rows, 128))

    def normalise(load_rows, n_rows, rs_ref, a_ref, b_ref):
        def body(i, _):
            at = pl.ds(pl.multiple_of(i * 16, 16), 16)
            x = load_rows(at).astype(F32)
            r = rs_ref[at, :]
            for k in range(width // 128):
                c = slice(128 * k, 128 * k + 128)
                xn[at, c] = (x[:, c] * r * a_ref[:, c] + b_ref[:, c]).astype(BF16)
            return 0

        lax.fori_loop(0, n_rows // 16, body, 0)

    row_scale(lambda at: ctx_v[at, :], 2 * ctx_tok, rsc)
    mods.pass_on(4)
    mods.pass_on(6)
    mods.finish()

    total = pm[0]
    for k in range(1, n_sp):
        total = total + pm[k]
    ms[tp] = total
    m_copies = []
    for k in range(1, n_tp):
        to = lax.rem(tp + k, n_tp)
        copy = remote(ms.at[tp], ms.at[tp], msend.at[k], mrecv.at[k], {"tp": to})
        copy.start()
        m_copies.append(copy)
    lat_x.send_own(1)
    for k in range(1, n_tp):
        source = lax.rem(tp + n_tp - k, n_tp)
        remote(ms.at[source], ms.at[source], msend.at[k], mrecv.at[k], {"tp": tp}).wait_recv()
    par = lax.rem(lax.broadcasted_iota(jnp.int32, (16, mod_cols), 0), 2) == 0
    for t in range(n_tp):
        c = slice(t * mod_cols, (t + 1) * mod_cols)
        m = ms[t]
        gain = gain_v[:, c]
        ac16[:, c] = jnp.broadcast_to(gain * (1.0 + m[5:6]), (16, mod_cols))
        bc16[:, c] = jnp.broadcast_to(m[2:3], (16, mod_cols))
        a16[:, c] = jnp.where(par, gain * (1.0 + m[3:4]), gain * (1.0 + m[4:5]))
        b16[:, c] = jnp.where(par, m[0:1], m[1:2])
        g16[:, c] = jnp.where(par, m[6:7], m[7:8])

    lane_lo = lax.broadcasted_iota(jnp.int32, (64, 128), 1) < HEAD_DIM
    normalise(lambda at: ctx_v[at, :], 2 * ctx_tok, rsc, ac16, bc16)
    tmp[...] = jnp.dot(xn[...], w_all[:, 128:256], preferred_element_type=F32)
    for s in range(2):
        ck[s, pl.ds(pl.multiple_of(sp * ctx_tok, ctx_tok), ctx_tok), :] = tmp[
            pl.ds(s, ctx_tok, stride=2), :
        ].astype(BF16)
    ctxs.pass_on(0)

    lane = lax.broadcasted_iota(jnp.int32, (rows, 128), 1)
    first_half = lax.rem(lane, HEAD_DIM) < HEAD_DIM // 2

    def rotate(v, cos, sin):
        swapped = jnp.where(first_half, pltpu.roll(v, 128 - HEAD_DIM // 2, 1), pltpu.roll(v, HEAD_DIM // 2, 1))
        return v * cos + swapped * sin

    def one_block(b):
        row_scale(lambda at: lat_all[b, at, :], rows, rsb)
        normalise(lambda at: lat_all[b, at, :], rows, rsb, a16, b16)
        proj = jnp.dot(xn[...], w_all[...], preferred_element_type=F32)
        at_q = pl.ds(pl.multiple_of(b * local_tok, local_tok), local_tok)
        at_k = pl.ds(pl.multiple_of(b * local_tok + WINDOW, local_tok), local_tok)
        r = [row_v[k, pl.ds(b, 1), :] for k in range(4)]
        tmp[...] = rotate(proj[:, 0:128], col_v[0] + r[0], col_v[1] + r[1])
        for s in range(2):
            v = tmp[pl.ds(s, local_tok, stride=2), :]
            q_s[s, 0, at_q, :] = jnp.where(lane_lo, v, 0.0).astype(BF16)
            q_s[s, 1, at_q, :] = jnp.where(lane_lo, pltpu.roll(v, 64, 1), 0.0).astype(BF16)
        tmp[...] = rotate(proj[:, 128:256], col_v[2] + r[2], col_v[3] + r[3])
        for s in range(2):
            v = tmp[pl.ds(s, local_tok, stride=2), :]
            kv_s[s, at_k, :] = v.astype(BF16)
            vv_s[s, at_k, :] = jnp.where(lane_lo, 1.0, v).astype(BF16)

    def chip_blocks(x):
        def body(j, _):
            one_block(x * 2 + j)
            return 0

        lax.fori_loop(0, 2, body, 0)

    lat_x.pass_near()
    wo_x.send_own(0)
    lat_x.land_shared("own2")
    chip_blocks(lat_x.x)
    ctxs.pass_on(2)
    lat_x.land_shared("left2")
    chip_blocks(lat_x.left_x)
    ctxs.pass_on(4)
    lat_x.land_shared("right2")
    chip_blocks(lat_x.right_x)
    lat_x.pass_far()
    ctxs.pass_on(6)
    lat_x.land_shared("far2")
    chip_blocks(lat_x.far_x)

    up, down = lax.rem(sp + 1, n_sp), lax.rem(sp + n_sp - 1, n_sp)
    to_down = remote(
        kv_s.at[:, pl.ds(WINDOW, WINDOW), :], kv_s.at[:, pl.ds(tokens + WINDOW, WINDOW), :],
        hsend.at[0], hrecv.at[0], {"sp": down},
    )
    to_up = remote(
        kv_s.at[:, pl.ds(tokens, WINDOW), :], kv_s.at[:, pl.ds(0, WINDOW), :], hsend.at[1], hrecv.at[1], {"sp": up}
    )
    to_down.start()
    to_up.start()
    wo_x.pass_near()
    to_down.wait_recv()
    to_up.wait_recv()
    edge_lo = lax.broadcasted_iota(jnp.int32, (WINDOW, 128), 1) < HEAD_DIM
    one = jnp.ones((WINDOW, 128), BF16)
    for s in range(2):
        for at in (0, tokens + WINDOW):
            vv_s[s, at : at + WINDOW, :] = jnp.where(edge_lo, one, kv_s[s, at : at + WINDOW, :])

    q_rows = WINDOW
    n_q = tokens // q_rows
    heads = q_s.shape[1]
    stack = heads * q_rows
    span = q_rows + 2 * WINDOW
    row_i = lax.broadcasted_iota(jnp.int32, (stack, span), 0)
    i_q = lax.rem(row_i, q_rows)
    j_k = lax.broadcasted_iota(jnp.int32, (stack, span), 1)
    first_head = lax.broadcasted_iota(jnp.int32, (stack, 128), 0) < q_rows
    sink = jnp.where(first_head, sink_ref[0] * LOG2E, sink_ref[1] * LOG2E)
    sum_lane = lax.broadcasted_iota(jnp.int32, (stack, 128), 1) < HEAD_DIM

    def scores(q, k):
        return lax.dot_general(q, k, (((1,), (1,)), ((), ())), preferred_element_type=F32)

    def window_block(it, _):
        s = it // n_q
        qb = lax.rem(it, n_q)
        at_q = pl.ds(pl.multiple_of(qb * q_rows, q_rows), q_rows)
        at_k = pl.ds(pl.multiple_of(qb * q_rows, q_rows), span)
        q = q_s[s, :, at_q, :].reshape(stack, 128)
        first_key = sp * tokens + qb * q_rows - WINDOW
        lo = jnp.maximum(i_q, -first_key)
        hi = jnp.minimum(i_q + 2 * WINDOW, seq_length - 1 - first_key)
        sc = jnp.where((j_k >= lo) & (j_k <= hi), scores(q, kv_s[s, at_k, :]), BIG_NEG)
        top = jnp.maximum(jnp.max(sc, axis=-1, keepdims=True), sink)
        p = jnp.exp2(sc - top[:, 0:1]).astype(BF16)
        o = jnp.dot(p, vv_s[s, at_k, :], preferred_element_type=F32)
        o_s[it] = o + jnp.where(sum_lane, jnp.exp2(sink - top), 0.0)
        m_s[it] = top
        return 0

    lax.fori_loop(0, 2 * n_q, window_block, 0)

    ctxs.finish()
    n_ctx = ck.shape[1]
    ctx_lo = lax.broadcasted_iota(jnp.int32, (n_ctx, 128), 1) < HEAD_DIM
    for s in range(2):
        cv[s] = jnp.where(ctx_lo, jnp.ones((n_ctx, 128), BF16), ck[s])
    out_lo = lax.broadcasted_iota(jnp.int32, (q_rows, 128), 1) < HEAD_DIM

    def a_copy(b):
        return remote(
            asend.at[b], att_all.at[tp], asem.at[b], arecv.at[tp], {"tp": b}
        )

    per_q = q_rows // local_tok

    def ctx_block(qb, _):
        for s in range(2):
            it = s * n_q + qb
            at_q = pl.ds(pl.multiple_of(qb * q_rows, q_rows), q_rows)
            q = q_s[s, :, at_q, :].reshape(stack, 128)
            sc = scores(q, ck[s])
            old = m_s[it]
            top = jnp.maximum(jnp.max(sc, axis=-1, keepdims=True), old)
            p = jnp.exp2(sc - top[:, 0:1]).astype(BF16)
            o = jnp.dot(p, cv[s], preferred_element_type=F32) + o_s[it] * jnp.exp2(old - top)
            r = o / pltpu.roll(o, 64, 1)
            tmp2[pl.ds(s, q_rows, stride=2), :] = jnp.where(
                out_lo, pltpu.roll(r[0:q_rows], 64, 1), r[q_rows:stack]
            )
        for k in range(per_q):
            asend[qb * per_q + k] = tmp2[k * rows : (k + 1) * rows, :].astype(BF16)
        for k in range(per_q):
            b = qb * per_q + k

            @pl.when(b != tp)
            def _():
                a_copy(b).start()

        return 0

    lax.fori_loop(0, n_q, ctx_block, 0)

    wo_x.pass_far()
    att_all[tp] = asend[tp]
    for k in range(1, n_tp):
        source = lax.rem(tp + k, n_tp)
        remote(
            asend.at[0], att_all.at[source], asem.at[0], arecv.at[source], {"tp": tp}
        ).wait_recv()
    for name in ("own2", "left2", "right2", "far2"):
        wo_x.land_shared(name)

    att = jnp.concatenate([att_all[t] for t in range(n_tp)], axis=1)
    tile = 256

    def out_block(n, _):
        c = pl.ds(pl.multiple_of(n * tile, tile), tile)
        w = wo_all[:, :, c].reshape(n_tp * rows, tile)
        mixed = jnp.dot(att, w, preferred_element_type=F32)
        gated = (mixed.reshape(rows // 16, 16, tile) * g16[:, c][None]).reshape(rows, tile)
        out_ref[:, c] = (lat_all[tp, :, c].astype(F32) + gated).astype(BF16)
        return 0

    lax.fori_loop(0, width // tile, out_block, 0)

    mods.drain()
    ctxs.drain()
    lat_x.drain()
    wo_x.drain()
    for copy in m_copies:
        copy.wait_send()
    to_down.wait_send()
    to_up.wait_send()
    for b in range(n_tp):

        @pl.when(b != tp)
        def _():
            a_copy(b).wait_send()


def on_device(n_sp, n_tp, latents, context, condition, cond_context, w_shift, w_scale, w_gate, norm_gain, w_query,
              w_key, w_value, sink_logit, w_out):
    local_tok, samples, width = latents.shape
    ctx_tok = context.shape[0]
    rows, ctx_rows = local_tok * samples, ctx_tok * samples
    tokens = local_tok * n_tp
    n_ctx = ctx_tok * n_sp
    mod_cols = w_shift.shape[1]
    heads = w_query.shape[1] // HEAD_DIM
    assert samples == 2 and local_tok == GRID_W and heads == 2 and w_key.shape[1] == HEAD_DIM
    assert w_out.shape[0] == rows == ctx_rows == 128
    col_tab, row_tab = rope_tables(tokens * n_sp // GRID_W)
    n_blocks = tokens // WINDOW
    any_spec = pl.BlockSpec(memory_space=pl.ANY)
    n_l = RingOfChips.count((0, 0))
    n_w = RingOfChips.count((0,))
    dma = pltpu.SemaphoreType.DMA
    scratch = [
        pltpu.VMEM((n_tp, rows, width), BF16),
        pltpu.VMEM((n_tp, rows, width), BF16),
        pltpu.VMEM((ctx_rows, width), BF16),
        pltpu.VMEM(condition.shape, F32),
        pltpu.VMEM((1, cond_context.shape[0]), F32),
        pltpu.VMEM((3, *w_shift.shape), BF16),
        pltpu.VMEM((1, width), F32),
        pltpu.VMEM((width, 256), BF16),
        pltpu.VMEM((128, width), BF16),
        pltpu.VMEM((4, rows, 128), F32),
        pltpu.VMEM((4, n_tp, 128), F32),
        pltpu.VMEM((n_sp, 8, mod_cols), F32),
        pltpu.VMEM((n_tp, 8, mod_cols), F32),
        *[pltpu.VMEM((16, width), F32) for _ in range(5)],
        *[pltpu.VMEM((rows, 128), F32) for _ in range(3)],
        pltpu.VMEM((rows, width), BF16),
        pltpu.VMEM((rows, 128), F32),
        pltpu.VMEM((2, heads, tokens, 128), BF16),
        pltpu.VMEM((2, tokens + 2 * WINDOW, 128), BF16),
        pltpu.VMEM((2, tokens + 2 * WINDOW, 128), BF16),
        pltpu.VMEM((2, n_ctx, 128), BF16),
        pltpu.VMEM((2, n_ctx, 128), BF16),
        pltpu.VMEM((2 * n_blocks, heads * WINDOW, 128), F32),
        pltpu.VMEM((2 * n_blocks, heads * WINDOW, 128), F32),
        pltpu.VMEM((2 * WINDOW, 128), F32),
        pltpu.VMEM((n_tp, rows, 128), BF16),
        pltpu.VMEM((n_tp, rows, 128), BF16),
        dma((14,)),
        dma((2, n_sp)), dma((2, n_sp)),
        dma((n_l,)), dma((n_l,)),
        dma((n_w,)), dma((n_w,)),
        dma((n_tp,)), dma((n_tp,)),
        dma((2,)), dma((2,)),
        dma((n_tp,)), dma((n_tp,)),
    ]
    out = pl.pallas_call(
        functools.partial(kernel, n_sp, n_tp, tokens * n_sp),
        out_shape=jax.ShapeDtypeStruct((rows, width), BF16),
        in_specs=[any_spec] * 11 + [pl.BlockSpec(memory_space=pltpu.SMEM)] + [any_spec] * 3,
        out_specs=pl.BlockSpec(memory_space=pltpu.VMEM),
        scratch_shapes=scratch,
        compiler_params=pltpu.CompilerParams(
            collective_id=0, has_side_effects=True, vmem_limit_bytes=60 * 1024 * 1024
        ),
    )(
        latents.reshape(rows, width),
        context.reshape(ctx_rows, width),
        condition,
        cond_context[None, :],
        w_shift,
        w_scale,
        w_gate,
        norm_gain[None, :],
        w_query,
        w_key.T,
        w_value.T,
        sink_logit,
        w_out,
        jnp.asarray(col_tab),
        jnp.asarray(row_tab),
    )
    return out.reshape(local_tok, samples, width)


def solution(mesh):
    n_sp, n_tp = mesh.shape["sp"], mesh.shape["tp"]
    sp_tp = ("sp", "tp")
    return jax.shard_map(
        functools.partial(on_device, n_sp, n_tp),
        mesh=mesh,
        in_specs=(
            P(sp_tp, "grp", None),
            P("sp", "grp", None),
            P("grp", "sp"),
            P("sp"),
            P("sp", "tp"),
            P("sp", "tp"),
            P("sp", "tp"),
            P(),
            P(None, "tp"),
            P(None, "tp"),
            P(None, "tp"),
            P("tp"),
            P("tp", None),
        ),
        out_specs=P(sp_tp, "grp", None),
        check_vma=False,
    )
```

time: 154 us -> 86.6 us (0.56)
  Pallas kernels: 0 us -> 80.4 us
  blocking collectives: 53.8 us -> 0 us
  starting transfers between devices: 33.8 us -> 0 us
  matrix products: 16.6 us -> 0 us
  waiting for transfers between devices: 15.8 us -> 0 us
  between operations: 13.8 us -> 0.01 us
  other arithmetic: 10.3 us -> 0 us
  local copies, waits for them, and re-layouts: 8.78 us -> 5.25 us
    pallas_call x0 -> x1, Pallas kernels: none -> 80.4 us  [on_device(): pl.pallas_call(functools.partial(kernel, n_sp, n_tp, tokens * n_sp), out_...]
    all_gather x2 -> x0, blocking collectives: 43.4 us -> none  [the longest x1 26 us: on_device(): lax.all_gather(jnp.dot(flat_ctx, w_pair, preferred_element_type=jnp.float...]
    all_to_all x2 -> x0, starting transfers between devices: 28.1 us -> none  [the longest x1 24.5 us: from_everyone(): return lax.all_to_all(copies, axis, split_axis=0, concat_axis=0, tiled=True)]
    dot_general x10 -> x0, matrix products: 16.6 us -> none  [the longest x1 3.48 us: on_device(): jnp.einsum('rgc,gcd->grd', grouped, w_groups, preferred_element_type=jnp....]
    all_to_all x1 -> x0, blocking collectives: 10.4 us -> none  [moved_by_axis(): lax.all_to_all(tiles, axes[k], split_axis=k, concat_axis=k, tiled=True)]
    all_to_all x2 -> x0, waiting for transfers between devices: 9.62 us -> none  [the longest x1 9.2 us: from_everyone(): return lax.all_to_all(copies, axis, split_axis=0, concat_axis=0, tiled=True)]
    ppermute x2 -> x0, starting transfers between devices: 5.52 us -> none  [the longest x1 4.22 us: with_halo(): lax.ppermute(tail, axis, [(i, (i + 1) % count) for i in range(ends)])]
    reduce_sum x5 -> x0, other arithmetic: 5.43 us -> none  [the longest x2 2.57 us: modulate(): jnp.mean(upcast * upcast, axis=-1, keepdims=True) + EPS]
  transfers between devices with their start and end apart: 6 -> 0, of which waited for: 3 -> 0; matrix products, arithmetic and copies ran while one was open for 15% -> 0% of each run, Pallas kernels for 0% -> 0%
where the time goes in v1:
time: 86.6 us; the launch traced here: 85.7 us
  Pallas kernels  80.4 us (93%)
  local copies, waits for them, and re-layouts  5.25 us (6%)
    pallas_call x1, Pallas kernels, on_device(): pl.pallas_call(functools.partial(kernel, n_sp, n_tp, tokens * n_sp), out_...  80.4 us
    reshape x1, local copies, waits for them, and re-layouts, on_device(): return out.reshape(local_tok, samples, width)  2.17 us
    reshape x1, local copies, waits for them, and re-layouts, on_device(): latents.reshape(rows, width)  2.09 us

profile of v1, /device:TPU:33, one launch (start us, length us, event | category | flops | bytes accessed | tf_op | source)
XLA Modules:
  0.0 85.7 jit_solution(15507178743036299976)
XLA Ops:
  0.0 0.0 copy-start
  0.0 2.1 %reshape.9.lat_hbm = bf16[128,2048]{1,0:T(8,128)(2,1)} reshape(bf16[64,2,2048]{2,1,0:T(2,128)(2,1)} %param.15) | data formatting | bytes 1048576 | tf_op jit(solution)/shard_map/reshape | solution.py:569
  2.1 0.0 copy-done
  2.1 1.0 %reshape.10.ctx_hbm = bf16[128,2048]{1,0:T(8,128)(2,1)} reshape(bf16[64,2,2048]{2,1,0:T(2,128)(2,1)S(1)} %copy-done) | data formatting | bytes 1048576 | tf_op jit(solution)/shard_map/reshape | solution.py:570
  3.1 80.4 %shard_map.145 = bf16[128,2048]{1,0:T(8,128)(2,1)} custom-call(bf16[128,2048]{1,0:T(8,128)(2,1)} %reshape.9.lat_hbm, bf16[128,2048]{1,0:T(8,128)(2,1)} %reshape.10.ctx_hbm, f32[2,128]{1,0:T(2,128)} %cond_hbm.1, f32[1,128]{1,0:T(1,128)} %bitcast.7, bf16[128,256]{1,0:T(8,128)(2,1)} %wsh_hbm.1, bf16[128,256]{1,0:T(8,128)(2,1)} %wsc_hbm.1, ...), custom_call_target="tpu_custom_call" | custom-call | tf_op jit(solution)/shard_map/pallas_call | solution.py:559
  83.5 2.2 %reshape.11 = bf16[64,2,2048]{2,1,0:T(2,128)(2,1)} reshape(bf16[128,2048]{1,0:T(8,128)(2,1)} %shard_map.145) | data formatting | bytes 1048576 | tf_op jit(solution)/shard_map/reshape | solution.py:585
Async XLA Ops:
  0.0 2.1 %copy-start = (bf16[64,2,2048]{2,1,0:T(2,128)(2,1)S(1)}, bf16[64,2,2048]{2,1,0:T(2,128)(2,1)}, u32[]{:S(2)}) copy-start(bf16[64,2,2048]{2,1,0:T(2,128)(2,1)} %param.16) | copy-start | bytes 1572868
